TPU v7x, 32 devices: a whole 2x2x4 slice. The times are simulated.
32 devices in a mesh: ep: 8 (over z, x), tp: 4 (over y, core).
Axes of the slice: x: 2, y: 2, z: 4, core: 2. Of those that a mesh axis runs over, the one named last changes fastest.
Arguments:
- queries: bfloat16 [2048, 1024], P('ep', 'tp'), may hold values from -6 to 6
- keys: bfloat16 [2048, 256], P('ep', 'tp'), may hold values from -6 to 6
- values: bfloat16 [2048, 256], P('ep', 'tp'), may hold values from -6 to 6
- q_gain: float32 [64], replicated, may hold values from 1 to 6
- k_gain: float32 [64], replicated, may hold values from 1 to 6
- out_weight: bfloat16 [1024, 2048], P('tp'), may hold values from -0.1875 to 0.1875
- tokens: bfloat16 [1024, 2048], P(('ep', 'tp')), may hold values from -6 to 6
- ffn_gain: float32 [2048], replicated, may hold values from 0.1 to 1.9
- route: int32 [1024, 2], P(('ep', 'tp')), may hold values from 0 to 7, all different within a row; in each aligned block of 32 rows (0 to 31, 32 to 63, ...) at most 16 rows name the same one
- route_weight: float32 [1024, 2], P(('ep', 'tp')), may hold values from 0.1 to 1
- gate_weight: bfloat16 [8, 2048, 3584], P('ep', None, 'tp'), may hold values from -0.125 to 0.125
- up_weight: bfloat16 [8, 2048, 3584], P('ep', None, 'tp'), may hold values from -0.125 to 0.125
- down_weight: bfloat16 [8, 3584, 2048], P('ep', 'tp'), may hold values from -0.09375 to 0.09375
Outputs:
- mixer_out: bfloat16 [2048, 2048], P(('ep', 'tp'))
- mixed: bfloat16 [1024, 2048], P(('ep', 'tp'))
Inputs may be any that keep to these rules, and one draw needn't show every extreme that they name: `route`: each row names 2 different experts. In every device's aligned block of 32 rows no expert is named more than 16 times, and in some blocks some expert is named exactly 16 times.
All inputs are finite; a program needn't handle non-finite values.
Results may differ from a plain program's by a relative error of at most 0.013.
The roundings to bfloat16 on the way count: a program that leaves them out, or rounds other values in their place, can miss the bound.
Values may be sent and summed in bfloat16 or wider, within the bound.
A program may use at most 192 MiB of HBM per device.

v0:
```python
import functools
import math

import jax
import jax.numpy as jnp
from jax import lax
from jax.experimental import pallas as pl
from jax.experimental.pallas import tpu as pltpu
from jax.sharding import PartitionSpec as P

GRID_W = 64


EPS = 1e-06
THETA = 10000.0


def head_norm(vals, gain):
    vals = vals.astype(jnp.float32)
    return vals * lax.rsqrt(jnp.mean(vals * vals, axis=-1, keepdims=True) + EPS) * gain


def rotate(vals, positions):
    pairs = vals.shape[-1] // 2
    quarter = pairs // 2
    freqs = THETA ** (-jnp.arange(quarter, dtype=jnp.float32) / quarter)
    grid_row = (positions // GRID_W).astype(jnp.float32)
    grid_col = (positions % GRID_W).astype(jnp.float32)
    angle = jnp.concatenate([grid_row[:, None] * freqs, grid_col[:, None] * freqs], axis=-1)
    cosine = jnp.cos(angle)[:, None, :]
    sine = jnp.sin(angle)[:, None, :]
    split = vals.reshape(vals.shape[:-1] + (pairs, 2))
    first = split[..., 0]
    second = split[..., 1]
    turned = jnp.stack([first * cosine - second * sine, first * sine + second * cosine], axis=-1)
    return turned.reshape(vals.shape)


def local(
    queries,
    keys,
    values,
    q_gain,
    k_gain,
    out_weight,
    tokens,
    ffn_gain,
    route,
    route_weight,
    gate_weight,
    up_weight,
    down_weight,
):
    local_rows = queries.shape[0]
    head_size = q_gain.shape[0]
    query_heads = queries.shape[1] // head_size
    key_heads = keys.shape[1] // head_size
    group = query_heads // key_heads
    key_width = key_heads * head_size
    positions = lax.axis_index("ep") * local_rows + jnp.arange(local_rows, dtype=jnp.int32)
    rot_q = rotate(
        head_norm(queries.reshape(local_rows, query_heads, head_size), q_gain), positions
    ).astype(jnp.bfloat16)
    rot_q = rot_q.reshape(local_rows, key_heads, group, head_size)
    rot_k = rotate(
        head_norm(keys.reshape(local_rows, key_heads, head_size), k_gain), positions
    ).astype(jnp.bfloat16)
    joined = jnp.concatenate([rot_k.reshape(local_rows, key_width), values], axis=1)
    scale = head_size ** (-0.5)

    def fold_block(carry, block):
        highest, denom, numer = carry
        key_block = block[:, :key_width].reshape(-1, key_heads, head_size)
        value_block = block[:, key_width:].reshape(-1, key_heads, head_size)
        scores = (
            jnp.einsum("qkgd,skd->qkgs", rot_q, key_block, preferred_element_type=jnp.float32)
            * scale
        )
        new_high = jnp.maximum(highest, jnp.max(scores, axis=-1))
        shrink = jnp.exp(highest - new_high)
        expo = jnp.exp(scores - new_high[..., None])
        denom = denom * shrink + jnp.sum(expo, axis=-1)
        numer = numer * shrink[..., None] + jnp.einsum(
            "qkgs,skd->qkgd",
            expo.astype(jnp.bfloat16),
            value_block,
            preferred_element_type=jnp.float32,
        )
        return ((new_high, denom, numer), None)

    start_high = jnp.full((local_rows, key_heads, group), -1e30, jnp.float32)
    start_denom = jnp.zeros((local_rows, key_heads, group), jnp.float32)
    start_numer = jnp.zeros((local_rows, key_heads, group, head_size), jnp.float32)
    carry = (start_high, start_denom, start_numer)
    piece = lax.all_gather(joined, "ep", axis=0, tiled=True)
    length = piece.shape[0]
    size = length
    while size > 2048 and size % 2 == 0:
        size = size // 2
    blocks = piece.reshape(length // size, size, piece.shape[1])
    carry, _ = lax.scan(fold_block, carry, blocks)
    highest, denom, numer = carry
    attended = (
        (numer / denom[..., None]).astype(jnp.bfloat16).reshape(local_rows, query_heads * head_size)
    )
    own_rows = tokens.shape[0]
    width = tokens.shape[1]
    picks_row = route.shape[1]
    experts = lax.axis_size("ep")
    capacity = 2 * own_rows * picks_row // experts
    token_float = tokens.astype(jnp.float32)
    normed = (
        token_float
        * lax.rsqrt(jnp.mean(token_float * token_float, axis=-1, keepdims=True) + EPS)
        * ffn_gain
    ).astype(jnp.bfloat16)
    flat_route = route.reshape(-1)
    expert_hot = (flat_route[:, None] == jnp.arange(experts, dtype=jnp.int32)[None, :]).astype(
        jnp.int32
    )
    earlier = jnp.cumsum(expert_hot, axis=0) - expert_hot
    rank = jnp.sum(earlier * expert_hot, axis=1)
    slot = flat_route * capacity + rank
    pick_hot = (slot[:, None] == jnp.arange(experts * capacity, dtype=jnp.int32)[None, :]).astype(
        jnp.bfloat16
    )
    row_hot = jnp.sum(pick_hot.reshape(own_rows, picks_row, experts * capacity), axis=1)
    outgoing = jnp.einsum("rs,rd->sd", row_hot, normed, preferred_element_type=jnp.float32).astype(
        jnp.bfloat16
    )
    outgoing = outgoing.reshape(experts, capacity, width)
    gate_local = gate_weight[0]
    up_local = up_weight[0]
    down_local = down_weight[0]
    arrived = lax.all_to_all(outgoing, "ep", split_axis=0, concat_axis=0, tiled=True)
    sources = arrived.shape[0]
    items = arrived.shape[1]
    slot_rows = arrived.reshape(sources * items, width)
    piece = lax.all_gather(slot_rows, "tp", axis=0, tiled=True)
    gate = jnp.dot(piece, gate_local, preferred_element_type=jnp.float32)
    upper = jnp.dot(piece, up_local, preferred_element_type=jnp.float32)
    hidden = (jax.nn.silu(gate) * upper).astype(jnp.bfloat16)
    worked = jnp.dot(hidden, down_local, preferred_element_type=jnp.float32).reshape(
        -1, items, width
    )
    head_partial = jnp.dot(attended, out_weight, preferred_element_type=jnp.float32)
    mixer_sum, expert_sum = (
        lax.psum_scatter(
            head_partial.astype(jnp.bfloat16), "tp", scatter_dimension=0, tiled=True
        ).astype(jnp.float32),
        lax.psum_scatter(worked.astype(jnp.bfloat16), "tp", scatter_dimension=0, tiled=True).astype(
            jnp.float32
        ),
    )
    mixer_out = mixer_sum.astype(jnp.bfloat16)
    home = expert_sum.astype(jnp.bfloat16)
    back = lax.all_to_all(home, "ep", split_axis=0, concat_axis=0, tiled=True)
    copies = jnp.dot(
        pick_hot, back.reshape(experts * capacity, width), preferred_element_type=jnp.float32
    )
    weighted = route_weight[..., None] * copies.reshape(own_rows, picks_row, width)
    mixed = jnp.sum(weighted, axis=1).astype(jnp.bfloat16)
    return (mixer_out, mixed)


def rotation_freqs(head_size):
    quarter = head_size // 4
    freqs = THETA ** (-jnp.arange(quarter, dtype=jnp.float32) / quarter)
    return jnp.repeat(jnp.concatenate([freqs, freqs]), 2)[None, :]


def norm_rotate(vals, gain, cosine, sine):
    vals = vals * lax.rsqrt(jnp.mean(vals * vals, axis=-1, keepdims=True) + EPS) * gain
    size = vals.shape[-1]
    lane = lax.broadcasted_iota(jnp.int32, vals.shape, 1)
    up = jnp.concatenate([vals[:, 1:], vals[:, :1]], axis=1)
    down = jnp.concatenate([vals[:, size - 1 :], vals[:, : size - 1]], axis=1)
    swapped = jnp.where(lane % 2 == 0, up, down)
    return vals * cosine + swapped * sine


def fused_kernel(
    dims,
    q_ref,
    k_ref,
    v_ref,
    qg_ref,
    kg_ref,
    fr_ref,
    tok_ref,
    fg_ref,
    route_t_ref,
    rw_ref,
    gate_hbm,
    up_hbm,
    down_hbm,
    ow_hbm,
    mix_ref,
    out_ref,
    wgu,
    wd,
    wo,
    og,
    slots,
    hidden,
    part,
    rs1,
    half,
    rs2,
    home,
    back,
    kvs,
    qp,
    att,
    mpart,
    mrs1,
    mhalf,
    mrs2,
    w_sem,
    a2a_s,
    a2a_r,
    f1_s,
    f1_r,
    f2_s,
    f2_r,
    f3_s,
    f3_r,
    kva_s,
    kva_r,
    kvb_s,
    kvb_r,
    r1_s,
    r1_r,
    r2_s,
    r2_r,
    bk_s,
    bk_r,
    m1_s,
    m1_r,
    m2_s,
    m2_r,
):
    ep, tp, cap, groups, tile = dims
    f32, bf16 = jnp.float32, jnp.bfloat16
    per = ep // groups
    e = lax.axis_index("ep")
    t = lax.axis_index("tp")
    t1 = t + 1 - 2 * (t % 2)
    t2 = (t + 2) % tp
    e1 = e + 1 - 2 * (e % 2)
    own_rows, width = tok_ref.shape
    head_size, rows = k_ref.shape
    heads = q_ref.shape[1] // head_size
    units = hidden.shape[1]
    lane_tile = wgu.shape[2] // 2

    def remote(src, dst, ssem, rsem, pe, pt):
        return pltpu.make_async_remote_copy(
            src_ref=src,
            dst_ref=dst,
            send_sem=ssem,
            recv_sem=rsem,
            device_id={"ep": pe, "tp": pt},
            device_id_type=pl.DeviceIdType.MESH,
        )

    barrier = pltpu.get_barrier_semaphore()
    peers = [((e + d) % ep, t) for d in range(1, ep)] + [(e, t1), (e, t2)]
    for pe, pt in peers:
        pl.semaphore_signal(
            barrier, inc=1, device_id={"ep": pe, "tp": pt}, device_id_type=pl.DeviceIdType.MESH
        )

    weights = []
    for n in range(units // lane_tile):
        cols = pl.ds(n * lane_tile, lane_tile)
        weights.append(
            pltpu.make_async_copy(
                gate_hbm.at[0, :, cols], wgu.at[n, :, pl.ds(0, lane_tile)], w_sem.at[2 * n]
            )
        )
        weights.append(
            pltpu.make_async_copy(
                up_hbm.at[0, :, cols],
                wgu.at[n, :, pl.ds(lane_tile, lane_tile)],
                w_sem.at[2 * n + 1],
            )
        )
    last = 2 * (units // lane_tile)
    weights.append(pltpu.make_async_copy(down_hbm.at[0], wd, w_sem.at[last]))
    load_out = pltpu.make_async_copy(ow_hbm, wo, w_sem.at[last + 1])
    for copy in weights:
        copy.start()
    load_out.start()

    position = e * rows + lax.broadcasted_iota(jnp.int32, (rows, head_size), 0)
    channel = lax.broadcasted_iota(jnp.int32, (rows, head_size), 1)
    grid_row = position // GRID_W
    place = jnp.where(channel < head_size // 2, grid_row, position - grid_row * GRID_W)
    angle = place.astype(f32) * fr_ref[...]
    cosine = jnp.cos(angle)
    sine = jnp.sin(angle) * jnp.where(channel % 2 == 0, -1.0, 1.0)
    both = jnp.concatenate([k_ref[...], v_ref[...]], axis=0).astype(f32).T
    rot_k = norm_rotate(both[:, :head_size], kg_ref[...], cosine, sine)
    kvs[0, 0, :, pl.ds(0, head_size)] = rot_k.astype(bf16)
    kvs[0, 0, :, pl.ds(head_size, head_size)] = both[:, head_size:].astype(bf16)

    slot_rows = ep * cap
    later = lax.broadcasted_iota(jnp.int32, (own_rows, own_rows), 0)
    early = lax.broadcasted_iota(jnp.int32, (own_rows, own_rows), 1)
    picks = []
    sends = jnp.zeros((slot_rows, own_rows), f32)
    topk = route_t_ref.shape[0]
    diag = later == early

    def column(row):
        return jnp.sum(jnp.where(diag, row, jnp.zeros_like(row)), axis=1, keepdims=True)

    columns = [column(route_t_ref[k : k + 1, :]) for k in range(topk)]
    for k in range(topk):
        col = columns[k]
        row = route_t_ref[k : k + 1, :]
        rank_col = jnp.zeros((own_rows, 1), f32)
        rank_row = jnp.zeros((1, own_rows), f32)
        for other in range(topk):
            same = (col == route_t_ref[other : other + 1, :]) & (early < later)
            rank_col += jnp.sum(jnp.where(same, 1.0, 0.0), axis=1, keepdims=True)
            same_t = (columns[other] == row) & (later < early)
            rank_row += jnp.sum(jnp.where(same_t, 1.0, 0.0), axis=0, keepdims=True)
        rel_col = jnp.where(col >= e, col - e, col - e + ep)
        rel_row = jnp.where(row >= e, row - e, row - e + ep)
        slot_col = (rel_col * cap).astype(f32) + rank_col
        slot_row = (rel_row * cap).astype(f32) + rank_row
        lanes = lax.broadcasted_iota(jnp.int32, (own_rows, slot_rows), 1).astype(f32)
        picks.append(jnp.where(lanes == slot_col, 1.0, 0.0).astype(bf16))
        subs = lax.broadcasted_iota(jnp.int32, (slot_rows, own_rows), 0).astype(f32)
        sends += jnp.where(subs == slot_row, 1.0, 0.0)
    tok = tok_ref[...].astype(f32)
    normed = (
        tok * lax.rsqrt(jnp.mean(tok * tok, axis=-1, keepdims=True) + EPS) * fg_ref[...]
    ).astype(bf16)
    outgoing = (
        jnp.dot(sends.astype(bf16), normed, preferred_element_type=f32)
        .astype(bf16)
        .reshape(ep, cap, width)
    )
    og[...] = outgoing
    slots[0, 0, 0] = outgoing[0]

    pl.semaphore_wait(barrier, len(peers))

    half_ep = ep // 2
    kva = {}
    kvb = {}
    for k in range(half_ep):
        kvb[k] = remote(kvs.at[0, k], kvs.at[1, k], kvb_s.at[k], kvb_r.at[k], e1, t)
        if k:
            kva[k] = remote(
                kvs.at[0, 0], kvs.at[0, k], kva_s.at[k], kva_r.at[k], (e + 2 * k) % ep, t
            )
    a2a = {}
    f1, f2, f3 = {}, {}, {}
    for d in range(ep):
        g, m = d // per, d % per
        if d:
            a2a[d] = remote(
                og.at[d], slots.at[g, 0, m], a2a_s.at[d], a2a_r.at[d], (e + d) % ep, t
            )
            a2a[d].start()
        f1[d] = remote(
            slots.at[g, 0, m], slots.at[g, 1, m], f1_s.at[d], f1_r.at[d], e, t1
        )
        f2[d] = remote(
            slots.at[g, 0, m], slots.at[g, 2, m], f2_s.at[d], f2_r.at[d], e, t2
        )
        f3[d] = remote(
            slots.at[g, 2, m], slots.at[g, 3, m], f3_s.at[d], f3_r.at[d], e, t1
        )

    for copy in kva.values():
        copy.start()
    kvb[0].start()

    def forward(d):
        if d:
            a2a[d].wait_recv()
        f2[d].start()
        f1[d].start()

    def relay(d):
        f2[d].wait_recv()
        f3[d].start()

    forward(0)

    for h in range(heads):
        lanes = pl.ds(h * head_size, head_size)
        turned = norm_rotate(q_ref[:, lanes].astype(f32), qg_ref[...], cosine, sine)
        qp[h, :, pl.ds(0, head_size)] = turned.astype(bf16)
        qp[h, :, pl.ds(head_size, head_size)] = jnp.zeros((rows, head_size), bf16)

    for d in range(1, ep):
        forward(d)

    def share_keys():
        for k in range(1, half_ep):
            kva[k].wait_recv()
            kvb[k].start()

    scale = head_size ** (-0.5) * math.log2(math.e)

    def attend(h):
        joined = kvs[...].reshape(ep * rows, 2 * head_size)
        scores = lax.dot_general(
            qp[h], joined, (((1,), (1,)), ((), ())), preferred_element_type=f32
        )
        expo = jnp.exp2((scores - jnp.max(scores, axis=-1, keepdims=True)) * scale)
        denom = jnp.sum(expo, axis=-1, keepdims=True)
        numer = jnp.dot(expo.astype(bf16), joined, preferred_element_type=f32)
        att[:, pl.ds(h * head_size, head_size)] = (numer[:, head_size:] / denom).astype(bf16)

    mrows = rows // tp
    homes = [t, t1, t2, (t1 + 2) % tp]
    m1 = [
        remote(mpart.at[2 * i + 1], mrs1.at[i], m1_s.at[i], m1_r.at[i], e, t1) for i in range(2)
    ]
    m2 = remote(mhalf, mrs2, m2_s, m2_r, e, t2)

    def project():
        for j in (3, 1, 2, 0):
            piece = att[pl.ds(pl.multiple_of(homes[j] * mrows, mrows), mrows), :]
            mpart[j] = jnp.dot(piece, wo[...], preferred_element_type=f32).astype(bf16)
            if j % 2:
                m1[j // 2].start()

    def feed(g):
        rows_g = tp * per * cap
        for d in range(g * per, (g + 1) * per):
            f1[d].wait_recv()
            f3[d].wait_recv()

        def up_step(n, carry):
            chosen = slots[g].reshape(rows_g, width)
            both = jnp.dot(chosen, wgu[n], preferred_element_type=f32)
            gate = both[:, :lane_tile]
            act = gate / (1.0 + jnp.exp(-gate)) * both[:, lane_tile:]
            hidden[:, pl.ds(pl.multiple_of(n * lane_tile, lane_tile), lane_tile)] = act.astype(
                bf16
            )
            return carry

        lax.fori_loop(0, units // lane_tile, up_step, 0)

        def down_step(n, carry):
            cols = pl.ds(pl.multiple_of(n * tile, tile), tile)
            result = jnp.dot(hidden[...], wd[:, cols], preferred_element_type=f32)
            part[g, :, :, :, cols] = result.astype(bf16).reshape(tp, per, cap, tile)
            return carry

        lax.fori_loop(0, width // tile, down_step, 0)

    r1, r2 = {}, {}
    for g in range(groups):
        for i in range(2):
            r1[g, i] = remote(
                part.at[g, 2 * i + 1], rs1.at[g, i], r1_s.at[g, i], r1_r.at[g, i], e, t1
            )
        r2[g] = remote(half.at[g], rs2.at[g], r2_s.at[g], r2_r.at[g], e, t2)
    bk = {}
    for d in range(1, ep):
        g, m = d // per, d % per
        bk[d] = remote(home.at[g, m], back.at[d], bk_s.at[d], bk_r.at[d], (e + ep - d) % ep, t)

    def pair_sum(g):
        r1[g, 1].wait_recv()
        half[g] = (part[g, 2].astype(f32) + rs1[g, 1].astype(f32)).astype(bf16)
        r2[g].start()

    def finish(g):
        r1[g, 0].wait_recv()
        r2[g].wait_recv()
        total = (
            part[g, 0].astype(f32) + rs1[g, 0].astype(f32) + rs2[g].astype(f32)
        ).astype(bf16)
        home[g] = total
        if g == 0:
            back[0] = total[0]
        for d in range(g * per, (g + 1) * per):
            if d:
                bk[d].start()

    def mixer_half():
        m1[1].wait_recv()
        mhalf[...] = (mpart[2].astype(f32) + mrs1[1].astype(f32)).astype(bf16)
        m2.start()

    for g in range(groups):
        for d in range(g * per, (g + 1) * per):
            relay(d)
        if g == 0:
            for copy in weights:
                copy.wait()
        feed(g)
        r1[g, 1].start()
        r1[g, 0].start()
        if g:
            pair_sum(g - 1)
        if g == groups // 2 - 1:
            share_keys()
    for k in range(half_ep):
        kvb[k].wait_recv()
    attend(0)
    pair_sum(groups - 1)
    for h in range(1, heads):
        if h < groups:
            finish(h - 1)
        attend(h)
    load_out.wait()
    project()
    for g in range(min(heads, groups) - 1, groups - 1):
        finish(g)
    mixer_half()
    finish(groups - 1)
    m1[0].wait_recv()
    m2.wait_recv()
    mix_ref[...] = (
        mpart[0].astype(f32) + mrs1[0].astype(f32) + mrs2[...].astype(f32)
    ).astype(bf16)
    for d in range(1, ep):
        bk[d].wait_recv()
    returned = back[...].reshape(slot_rows, width)
    mixed = jnp.zeros((own_rows, width), f32)
    for k in range(topk):
        mixed += column(rw_ref[k : k + 1, :]) * jnp.dot(
            picks[k], returned, preferred_element_type=f32
        )
    out_ref[...] = mixed.astype(bf16)

    for group in (kva, kvb, a2a, f1, f2, f3, r1, r2, bk):
        for copy in group.values():
            copy.wait_send()
    for copy in m1 + [m2]:
        copy.wait_send()


def local_fused(
    queries,
    keys,
    values,
    q_gain,
    k_gain,
    out_weight,
    tokens,
    ffn_gain,
    route,
    route_weight,
    gate_weight,
    up_weight,
    down_weight,
):
    ep = lax.axis_size("ep")
    tp = lax.axis_size("tp")
    rows = queries.shape[0]
    head_size = q_gain.shape[0]
    heads = queries.shape[1] // head_size
    own_rows, width = tokens.shape
    cap = 2 * own_rows * route.shape[1] // ep
    units = gate_weight.shape[2]
    lane_tile = 128
    tile = math.gcd(width, 512)
    groups = GROUPS
    per = ep // groups
    bf16 = jnp.bfloat16
    vmem = pl.BlockSpec(memory_space=pltpu.VMEM)
    hbm = pl.BlockSpec(memory_space=pl.ANY)
    dma = pltpu.SemaphoreType.DMA
    mrows = rows // tp
    flops = 2 * tp * ep * cap * width * units * 3 + 4 * heads * rows * rows * ep * head_size
    return pl.pallas_call(
        functools.partial(fused_kernel, (ep, tp, cap, groups, tile)),
        out_shape=(
            jax.ShapeDtypeStruct((mrows, width), bf16),
            jax.ShapeDtypeStruct((own_rows, width), bf16),
        ),
        in_specs=[vmem] * 10 + [hbm] * 4,
        out_specs=(vmem, vmem),
        scratch_shapes=[
            pltpu.VMEM((units // lane_tile, width, 2 * lane_tile), bf16),
            pltpu.VMEM((units, width), bf16),
            pltpu.VMEM(out_weight.shape, bf16),
            pltpu.VMEM((ep, cap, width), bf16),
            pltpu.VMEM((groups, tp, per, cap, width), bf16),
            pltpu.VMEM((tp * per * cap, units), bf16),
            pltpu.VMEM((groups, tp, per, cap, width), bf16),
            pltpu.VMEM((groups, 2, per, cap, width), bf16),
            pltpu.VMEM((groups, per, cap, width), bf16),
            pltpu.VMEM((groups, per, cap, width), bf16),
            pltpu.VMEM((groups, per, cap, width), bf16),
            pltpu.VMEM((ep, cap, width), bf16),
            pltpu.VMEM((2, ep // 2, rows, 2 * head_size), bf16),
            pltpu.VMEM((heads, rows, 2 * head_size), bf16),
            pltpu.VMEM((rows, heads * head_size), bf16),
            pltpu.VMEM((tp, mrows, width), bf16),
            pltpu.VMEM((2, mrows, width), bf16),
            pltpu.VMEM((mrows, width), bf16),
            pltpu.VMEM((mrows, width), bf16),
            dma((2 * (units // lane_tile) + 2,)),
        ]
        + [dma((ep,))] * 8
        + [dma((ep // 2,))] * 4
        + [dma((groups, 2))] * 2
        + [dma((groups,))] * 2
        + [dma((ep,))] * 2
        + [dma((2,))] * 2
        + [dma, dma],
        compiler_params=pltpu.CompilerParams(
            collective_id=0, has_side_effects=True, vmem_limit_bytes=60 * 1024 * 1024
        ),
        cost_estimate=pl.CostEstimate(
            flops=flops, bytes_accessed=3 * 2 * width * units, transcendentals=0
        ),
    )(
        queries,
        keys.T,
        values.T,
        q_gain[None, :],
        k_gain[None, :],
        rotation_freqs(head_size),
        tokens,
        ffn_gain[None, :],
        route.T,
        route_weight.T,
        gate_weight,
        up_weight,
        down_weight,
        out_weight,
    )


GROUPS = 4


def step(*args):
    queries, keys, q_gain, tokens, route, gate_weight = (args[i] for i in (0, 1, 3, 6, 8, 10))
    ep, tp = lax.axis_size("ep"), lax.axis_size("tp")
    cap = 2 * tokens.shape[0] * route.shape[1] // ep
    fits = (
        tp == 4
        and ep % 2 == 0
        and ep % GROUPS == 0
        and cap % 16 == 0
        and keys.shape[1] == q_gain.shape[0]
        and gate_weight.shape[2] % 128 == 0
        and queries.shape[0] % (16 * tp) == 0
    )
    return local_fused(*args) if fits else local(*args)


def solution(mesh):
    placed = (
        P("ep", "tp"),
        P("ep", "tp"),
        P("ep", "tp"),
        P(),
        P(),
        P("tp", None),
        P(("ep", "tp"), None),
        P(),
        P(("ep", "tp"), None),
        P(("ep", "tp"), None),
        P("ep", None, "tp"),
        P("ep", None, "tp"),
        P("ep", "tp", None),
    )
    return jax.shard_map(
        step,
        mesh=mesh,
        in_specs=placed,
        out_specs=(P(("ep", "tp"), None), P(("ep", "tp"), None)),
        check_vma=False,
    )
```

profile of v0, /device:TPU:0, one launch (start us, length us, event | category | flops | bytes accessed | tf_op | source)
XLA Modules:
  0.0 65.6 jit_solution(5845633367788105883)
XLA Ops:
  0.6 0.1 pad_maximum_fusion
  0.7 0.1 broadcast_in_dim.14
  0.8 0.6 broadcast_in_dim_reshape.3.fr_ref
  1.4 60.9 %shard_map.140 = (bf16[64,2048]{1,0:T(8,128)(2,1)}, bf16[32,2048]{1,0:T(8,128)(2,1)}) custom-call(bf16[256,256]{1,0:T(8,128)(2,1)} %q_ref.1, bf16[64,256]{1,0:T(8,128)(2,1)} %bitcast.7, bf16[64,256]{1,0:T(8,128)(2,1)} %bitcast.8, f32[1,64]{1,0:T(1,128)} %bitcast.12, f32[1,64]{1,0:T(1,128)} %bitcast.13, f32[1,64]{1,0:T(1,128)} %broadcast_in_dim_reshape.3.fr_ref, ...), custom_call_target="tpu_custom_call" | custom-call | flops 6174015488 | bytes 11010048 | tf_op jit(solution)/shard_map/pallas_call | solution.py:579
  62.3 1.7 %copy.17 = bf16[64,2048]{1,0:T(8,128)(2,1)} copy(bf16[64,2048]{1,0:T(8,128)(2,1)} %get-tuple-element.4) | data formatting | bytes 524288
  64.0 1.6 %copy.18 = bf16[32,2048]{1,0:T(8,128)(2,1)} copy(bf16[32,2048]{1,0:T(8,128)(2,1)} %get-tuple-element.5) | data formatting | bytes 262144
  (1 shorter events, 0.0 us)
where the time goes:
time: 65.8 us; the launch traced here: 65.6 us
  Pallas kernels  60.9 us (93%)
  local copies, waits for them, and re-layouts  3.93 us (6%)
    pallas_call x1, Pallas kernels, local_fused(): pl.pallas_call(functools.partial(fused_kernel, (ep, tp, cap, groups, tile...  60.9 us
    unnamed x2, local copies, waits for them, and re-layouts  3.24 us

commit v1 on v0

--- a/solution.py
+++ b/solution.py
@@ -163,12 +163,6 @@
     return (mixer_out, mixed)
 
 
-def rotation_freqs(head_size):
-    quarter = head_size // 4
-    freqs = THETA ** (-jnp.arange(quarter, dtype=jnp.float32) / quarter)
-    return jnp.repeat(jnp.concatenate([freqs, freqs]), 2)[None, :]
-
-
 def norm_rotate(vals, gain, cosine, sine):
     vals = vals * lax.rsqrt(jnp.mean(vals * vals, axis=-1, keepdims=True) + EPS) * gain
     size = vals.shape[-1]
@@ -186,7 +180,6 @@
     v_ref,
     qg_ref,
     kg_ref,
-    fr_ref,
     tok_ref,
     fg_ref,
     route_t_ref,
@@ -243,16 +236,26 @@
     ep, tp, cap, groups, tile = dims
     f32, bf16 = jnp.float32, jnp.bfloat16
     per = ep // groups
+    order = peer_order(ep)
+    place = {mask: i for i, mask in enumerate(order)}
     e = lax.axis_index("ep")
     t = lax.axis_index("tp")
     t1 = t + 1 - 2 * (t % 2)
     t2 = (t + 2) % tp
-    e1 = e + 1 - 2 * (e % 2)
     own_rows, width = tok_ref.shape
     head_size, rows = k_ref.shape
     heads = q_ref.shape[1] // head_size
     units = hidden.shape[1]
     lane_tile = wgu.shape[2] // 2
+    half_ep = ep // 2
+
+    def peer(mask):
+        other, bit = e, 1
+        while bit < ep:
+            if mask & bit:
+                other = other + bit * (1 - 2 * ((e // bit) % 2))
+            bit *= 2
+        return other
 
     def remote(src, dst, ssem, rsem, pe, pt):
         return pltpu.make_async_remote_copy(
@@ -265,7 +268,7 @@
         )
 
     barrier = pltpu.get_barrier_semaphore()
-    peers = [((e + d) % ep, t) for d in range(1, ep)] + [(e, t1), (e, t2)]
+    peers = [(peer(mask), t) for mask in range(1, ep)] + [(e, t1), (e, t2)]
     for pe, pt in peers:
         pl.semaphore_signal(
             barrier, inc=1, device_id={"ep": pe, "tp": pt}, device_id_type=pl.DeviceIdType.MESH
@@ -293,18 +296,6 @@
         copy.start()
     load_out.start()
 
-    position = e * rows + lax.broadcasted_iota(jnp.int32, (rows, head_size), 0)
-    channel = lax.broadcasted_iota(jnp.int32, (rows, head_size), 1)
-    grid_row = position // GRID_W
-    place = jnp.where(channel < head_size // 2, grid_row, position - grid_row * GRID_W)
-    angle = place.astype(f32) * fr_ref[...]
-    cosine = jnp.cos(angle)
-    sine = jnp.sin(angle) * jnp.where(channel % 2 == 0, -1.0, 1.0)
-    both = jnp.concatenate([k_ref[...], v_ref[...]], axis=0).astype(f32).T
-    rot_k = norm_rotate(both[:, :head_size], kg_ref[...], cosine, sine)
-    kvs[0, 0, :, pl.ds(0, head_size)] = rot_k.astype(bf16)
-    kvs[0, 0, :, pl.ds(head_size, head_size)] = both[:, head_size:].astype(bf16)
-
     slot_rows = ep * cap
     later = lax.broadcasted_iota(jnp.int32, (own_rows, own_rows), 0)
     early = lax.broadcasted_iota(jnp.int32, (own_rows, own_rows), 1)
@@ -315,6 +306,12 @@
 
     def column(row):
         return jnp.sum(jnp.where(diag, row, jnp.zeros_like(row)), axis=1, keepdims=True)
+
+    def position_of(expert):
+        spot = jnp.zeros_like(expert)
+        for mask in range(ep):
+            spot += jnp.where(expert == peer(mask), place[mask], 0)
+        return spot
 
     columns = [column(route_t_ref[k : k + 1, :]) for k in range(topk)]
     for k in range(topk):
@@ -327,10 +324,8 @@
             rank_col += jnp.sum(jnp.where(same, 1.0, 0.0), axis=1, keepdims=True)
             same_t = (columns[other] == row) & (later < early)
             rank_row += jnp.sum(jnp.where(same_t, 1.0, 0.0), axis=0, keepdims=True)
-        rel_col = jnp.where(col >= e, col - e, col - e + ep)
-        rel_row = jnp.where(row >= e, row - e, row - e + ep)
-        slot_col = (rel_col * cap).astype(f32) + rank_col
-        slot_row = (rel_row * cap).astype(f32) + rank_row
+        slot_col = (position_of(col) * cap).astype(f32) + rank_col
+        slot_row = (position_of(row) * cap).astype(f32) + rank_row
         lanes = lax.broadcasted_iota(jnp.int32, (own_rows, slot_rows), 1).astype(f32)
         picks.append(jnp.where(lanes == slot_col, 1.0, 0.0).astype(bf16))
         subs = lax.broadcasted_iota(jnp.int32, (slot_rows, own_rows), 0).astype(f32)
@@ -345,53 +340,69 @@
         .reshape(ep, cap, width)
     )
     og[...] = outgoing
-    slots[0, 0, 0] = outgoing[0]
-
-    pl.semaphore_wait(barrier, len(peers))
-
-    half_ep = ep // 2
-    kva = {}
-    kvb = {}
+    slots[place[0] // per, 0, place[0] % per] = outgoing[place[0]]
+
+    with jax.named_scope("barrier"):
+        pl.semaphore_wait(barrier, len(peers))
+
+    a2a, f1, f2, f3 = {}, {}, {}, {}
+    for i in range(ep):
+        g, m = i // per, i % per
+        if order[i]:
+            a2a[i] = remote(
+                og.at[i], slots.at[g, 0, m], a2a_s.at[i], a2a_r.at[i], peer(order[i]), t
+            )
+        f1[i] = remote(slots.at[g, 0, m], slots.at[g, 1, m], f1_s.at[i], f1_r.at[i], e, t1)
+        f2[i] = remote(slots.at[g, 0, m], slots.at[g, 2, m], f2_s.at[i], f2_r.at[i], e, t2)
+        f3[i] = remote(slots.at[g, 2, m], slots.at[g, 3, m], f3_s.at[i], f3_r.at[i], e, t1)
+    kva, kvb = {}, {}
     for k in range(half_ep):
-        kvb[k] = remote(kvs.at[0, k], kvs.at[1, k], kvb_s.at[k], kvb_r.at[k], e1, t)
+        kvb[k] = remote(kvs.at[0, k], kvs.at[1, k], kvb_s.at[k], kvb_r.at[k], peer(1), t)
         if k:
             kva[k] = remote(
-                kvs.at[0, 0], kvs.at[0, k], kva_s.at[k], kva_r.at[k], (e + 2 * k) % ep, t
+                kvs.at[0, 0], kvs.at[0, k], kva_s.at[k], kva_r.at[k], peer(2 * k), t
             )
-    a2a = {}
-    f1, f2, f3 = {}, {}, {}
-    for d in range(ep):
-        g, m = d // per, d % per
-        if d:
-            a2a[d] = remote(
-                og.at[d], slots.at[g, 0, m], a2a_s.at[d], a2a_r.at[d], (e + d) % ep, t
-            )
-            a2a[d].start()
-        f1[d] = remote(
-            slots.at[g, 0, m], slots.at[g, 1, m], f1_s.at[d], f1_r.at[d], e, t1
-        )
-        f2[d] = remote(
-            slots.at[g, 0, m], slots.at[g, 2, m], f2_s.at[d], f2_r.at[d], e, t2
-        )
-        f3[d] = remote(
-            slots.at[g, 2, m], slots.at[g, 3, m], f3_s.at[d], f3_r.at[d], e, t1
-        )
-
+
+    near, far = issue_order(ep)
+    for mask in near:
+        a2a[place[mask]].start()
+
+    def forward(mask):
+        i = place[mask]
+        with jax.named_scope(f"fwd{mask}"):
+            if mask:
+                a2a[i].wait_recv()
+            f2[i].start()
+            f1[i].start()
+
+    def relay(mask):
+        i = place[mask]
+        with jax.named_scope(f"relay{mask}"):
+            f2[i].wait_recv()
+            f3[i].start()
+
+    forward(0)
+
+    position = e * rows + lax.broadcasted_iota(jnp.int32, (rows, head_size), 0)
+    channel = lax.broadcasted_iota(jnp.int32, (rows, head_size), 1)
+    quarter = head_size // 4
+    power = (channel // 2) % quarter
+    freq = jnp.exp(power.astype(f32) * (-math.log(THETA) / quarter))
+    grid_row = position // GRID_W
+    spot = jnp.where(channel < head_size // 2, grid_row, position - grid_row * GRID_W)
+    angle = spot.astype(f32) * freq
+    cosine = jnp.cos(angle)
+    sine = jnp.sin(angle) * jnp.where(channel % 2 == 0, -1.0, 1.0)
+    both = jnp.concatenate([k_ref[...], v_ref[...]], axis=0).astype(f32).T
+    rot_k = norm_rotate(both[:, :head_size], kg_ref[...], cosine, sine)
+    kvs[0, 0, :, pl.ds(0, head_size)] = rot_k.astype(bf16)
+    kvs[0, 0, :, pl.ds(head_size, head_size)] = both[:, head_size:].astype(bf16)
+
+    for mask in far:
+        a2a[place[mask]].start()
     for copy in kva.values():
         copy.start()
     kvb[0].start()
-
-    def forward(d):
-        if d:
-            a2a[d].wait_recv()
-        f2[d].start()
-        f1[d].start()
-
-    def relay(d):
-        f2[d].wait_recv()
-        f3[d].start()
-
-    forward(0)
 
     for h in range(heads):
         lanes = pl.ds(h * head_size, head_size)
@@ -399,25 +410,34 @@
         qp[h, :, pl.ds(0, head_size)] = turned.astype(bf16)
         qp[h, :, pl.ds(head_size, head_size)] = jnp.zeros((rows, head_size), bf16)
 
-    for d in range(1, ep):
-        forward(d)
-
-    def share_keys():
-        for k in range(1, half_ep):
+    def share_keys(k):
+        with jax.named_scope(f"share{k}"):
             kva[k].wait_recv()
             kvb[k].start()
 
     scale = head_size ** (-0.5) * math.log2(math.e)
-
-    def attend(h):
+    half_rows = rows // 2
+    y = t // 2
+    stack = 2
+
+    def attend(side, h):
+        start = pl.multiple_of(side * half_rows, half_rows)
         joined = kvs[...].reshape(ep * rows, 2 * head_size)
+        chosen = qp[pl.ds(h, stack), pl.ds(start, half_rows), :]
         scores = lax.dot_general(
-            qp[h], joined, (((1,), (1,)), ((), ())), preferred_element_type=f32
+            chosen.reshape(stack * half_rows, 2 * head_size),
+            joined,
+            (((1,), (1,)), ((), ())),
+            preferred_element_type=f32,
         )
         expo = jnp.exp2((scores - jnp.max(scores, axis=-1, keepdims=True)) * scale)
         denom = jnp.sum(expo, axis=-1, keepdims=True)
         numer = jnp.dot(expo.astype(bf16), joined, preferred_element_type=f32)
-        att[:, pl.ds(h * head_size, head_size)] = (numer[:, head_size:] / denom).astype(bf16)
+        result = (numer[:, head_size:] / denom).astype(bf16)
+        for k in range(stack):
+            att[pl.ds(start, half_rows), pl.ds((h + k) * head_size, head_size)] = result[
+                k * half_rows : (k + 1) * half_rows
+            ]
 
     mrows = rows // tp
     homes = [t, t1, t2, (t1 + 2) % tp]
@@ -426,38 +446,38 @@
     ]
     m2 = remote(mhalf, mrs2, m2_s, m2_r, e, t2)
 
-    def project():
-        for j in (3, 1, 2, 0):
+    def project(js):
+        for j in js:
             piece = att[pl.ds(pl.multiple_of(homes[j] * mrows, mrows), mrows), :]
             mpart[j] = jnp.dot(piece, wo[...], preferred_element_type=f32).astype(bf16)
             if j % 2:
                 m1[j // 2].start()
 
-    def feed(g):
-        rows_g = tp * per * cap
-        for d in range(g * per, (g + 1) * per):
-            f1[d].wait_recv()
-            f3[d].wait_recv()
-
-        def up_step(n, carry):
+    def feed_wait(g):
+        with jax.named_scope(f"feedwait{g}"):
+            for i in range(g * per, (g + 1) * per):
+                f1[i].wait_recv()
+                f3[i].wait_recv()
+
+    rows_g = tp * per * cap
+
+    def up(g):
+        with jax.named_scope(f"up{g}"):
             chosen = slots[g].reshape(rows_g, width)
-            both = jnp.dot(chosen, wgu[n], preferred_element_type=f32)
-            gate = both[:, :lane_tile]
-            act = gate / (1.0 + jnp.exp(-gate)) * both[:, lane_tile:]
-            hidden[:, pl.ds(pl.multiple_of(n * lane_tile, lane_tile), lane_tile)] = act.astype(
-                bf16
-            )
-            return carry
-
-        lax.fori_loop(0, units // lane_tile, up_step, 0)
-
-        def down_step(n, carry):
-            cols = pl.ds(pl.multiple_of(n * tile, tile), tile)
-            result = jnp.dot(hidden[...], wd[:, cols], preferred_element_type=f32)
-            part[g, :, :, :, cols] = result.astype(bf16).reshape(tp, per, cap, tile)
-            return carry
-
-        lax.fori_loop(0, width // tile, down_step, 0)
+            for n in range(units // lane_tile):
+                both = jnp.dot(chosen, wgu[n], preferred_element_type=f32)
+                gate = both[:, :lane_tile]
+                act = gate / (1.0 + jnp.exp(-gate)) * both[:, lane_tile:]
+                hidden[:, pl.ds(n * lane_tile, lane_tile)] = act.astype(bf16)
+
+    def down(g):
+        with jax.named_scope(f"down{g}"):
+            for n in range(width // tile):
+                cols = pl.ds(n * tile, tile)
+                result = jnp.dot(hidden[...], wd[:, cols], preferred_element_type=f32)
+                part[g, :, :, :, cols] = result.astype(bf16).reshape(tp, per, cap, tile)
+        r1[g, 1].start()
+        r1[g, 0].start()
 
     r1, r2 = {}, {}
     for g in range(groups):
@@ -467,67 +487,104 @@
             )
         r2[g] = remote(half.at[g], rs2.at[g], r2_s.at[g], r2_r.at[g], e, t2)
     bk = {}
-    for d in range(1, ep):
-        g, m = d // per, d % per
-        bk[d] = remote(home.at[g, m], back.at[d], bk_s.at[d], bk_r.at[d], (e + ep - d) % ep, t)
+    for i in range(ep):
+        if order[i]:
+            bk[i] = remote(
+                home.at[i // per, i % per], back.at[i], bk_s.at[i], bk_r.at[i], peer(order[i]), t
+            )
 
     def pair_sum(g):
-        r1[g, 1].wait_recv()
-        half[g] = (part[g, 2].astype(f32) + rs1[g, 1].astype(f32)).astype(bf16)
-        r2[g].start()
+        with jax.named_scope(f"pairsum{g}"):
+            r1[g, 1].wait_recv()
+            half[g] = (part[g, 2].astype(f32) + rs1[g, 1].astype(f32)).astype(bf16)
+            r2[g].start()
 
     def finish(g):
-        r1[g, 0].wait_recv()
-        r2[g].wait_recv()
-        total = (
-            part[g, 0].astype(f32) + rs1[g, 0].astype(f32) + rs2[g].astype(f32)
-        ).astype(bf16)
-        home[g] = total
-        if g == 0:
-            back[0] = total[0]
-        for d in range(g * per, (g + 1) * per):
-            if d:
-                bk[d].start()
+        with jax.named_scope(f"finish{g}"):
+            r1[g, 0].wait_recv()
+            r2[g].wait_recv()
+            total = (
+                part[g, 0].astype(f32) + rs1[g, 0].astype(f32) + rs2[g].astype(f32)
+            ).astype(bf16)
+            home[g] = total
+            for i in range(g * per, (g + 1) * per):
+                if order[i]:
+                    bk[i].start()
+                else:
+                    back[i] = total[i % per]
 
     def mixer_half():
-        m1[1].wait_recv()
-        mhalf[...] = (mpart[2].astype(f32) + mrs1[1].astype(f32)).astype(bf16)
-        m2.start()
-
-    for g in range(groups):
-        for d in range(g * per, (g + 1) * per):
-            relay(d)
-        if g == 0:
-            for copy in weights:
-                copy.wait()
-        feed(g)
-        r1[g, 1].start()
-        r1[g, 0].start()
-        if g:
-            pair_sum(g - 1)
-        if g == groups // 2 - 1:
-            share_keys()
-    for k in range(half_ep):
-        kvb[k].wait_recv()
-    attend(0)
-    pair_sum(groups - 1)
-    for h in range(1, heads):
-        if h < groups:
-            finish(h - 1)
-        attend(h)
+        with jax.named_scope("mixhalf"):
+            m1[1].wait_recv()
+            mhalf[...] = (mpart[2].astype(f32) + mrs1[1].astype(f32)).astype(bf16)
+            m2.start()
+
+    forward(1)
+    forward(2)
+    relay(0)
+    relay(1)
+    forward(3)
+    forward(4)
+    relay(2)
+    for copy in weights:
+        copy.wait()
+    feed_wait(0)
+    up(0)
+    down(0)
+    relay(3)
+    forward(5)
+    relay(4)
+    forward(6)
+    forward(7)
+    feed_wait(1)
+    share_keys(1)
+    up(1)
+    pair_sum(0)
+    relay(5)
+    down(1)
+    relay(6)
+    share_keys(2)
+    feed_wait(2)
+    up(2)
+    relay(7)
+    pair_sum(1)
+    down(2)
+    share_keys(3)
+    feed_wait(3)
+    up(3)
+    pair_sum(2)
+    down(3)
+    finish(0)
+    pair_sum(3)
+    with jax.named_scope("kvwait"):
+        for k in range(half_ep):
+            kvb[k].wait_recv()
+    with jax.named_scope("att0"):
+        attend(1 - y, 0)
+    finish(1)
+    with jax.named_scope("att1"):
+        attend(1 - y, 2)
     load_out.wait()
-    project()
-    for g in range(min(heads, groups) - 1, groups - 1):
-        finish(g)
+    with jax.named_scope("project"):
+        project((3, 2))
+    finish(2)
+    with jax.named_scope("att2"):
+        attend(y, 0)
     mixer_half()
-    finish(groups - 1)
-    m1[0].wait_recv()
-    m2.wait_recv()
+    with jax.named_scope("att3"):
+        attend(y, 2)
+    finish(3)
+    with jax.named_scope("project"):
+        project((1, 0))
+    with jax.named_scope("mwait"):
+        m1[0].wait_recv()
+        m2.wait_recv()
     mix_ref[...] = (
         mpart[0].astype(f32) + mrs1[0].astype(f32) + mrs2[...].astype(f32)
     ).astype(bf16)
-    for d in range(1, ep):
-        bk[d].wait_recv()
+    with jax.named_scope("bkwait"):
+        for copy in bk.values():
+            copy.wait_recv()
     returned = back[...].reshape(slot_rows, width)
     mixed = jnp.zeros((own_rows, width), f32)
     for k in range(topk):
@@ -541,6 +598,25 @@
             copy.wait_send()
     for copy in m1 + [m2]:
         copy.wait_send()
+
+
+def peer_order(ep):
+    return tuple(range(1, ep)) + (0,)
+
+
+def issue_order(ep):
+    return tuple(range(1, ep)), ()
+
+
+def store_kernel(mix_ref, rows_ref, mix_out, rows_out, sems):
+    copies = [
+        pltpu.make_async_copy(mix_ref, mix_out, sems.at[0]),
+        pltpu.make_async_copy(rows_ref, rows_out, sems.at[1]),
+    ]
+    for copy in copies:
+        copy.start()
+    for copy in copies:
+        copy.wait()
 
 
 def local_fused(
@@ -576,13 +652,13 @@
     dma = pltpu.SemaphoreType.DMA
     mrows = rows // tp
     flops = 2 * tp * ep * cap * width * units * 3 + 4 * heads * rows * rows * ep * head_size
-    return pl.pallas_call(
+    held = pl.pallas_call(
         functools.partial(fused_kernel, (ep, tp, cap, groups, tile)),
         out_shape=(
-            jax.ShapeDtypeStruct((mrows, width), bf16),
-            jax.ShapeDtypeStruct((own_rows, width), bf16),
+            pltpu.VMEM((mrows, width), bf16),
+            pltpu.VMEM((own_rows, width), bf16),
         ),
-        in_specs=[vmem] * 10 + [hbm] * 4,
+        in_specs=[vmem] * 9 + [hbm] * 4,
         out_specs=(vmem, vmem),
         scratch_shapes=[
             pltpu.VMEM((units // lane_tile, width, 2 * lane_tile), bf16),
@@ -625,7 +701,6 @@
         values.T,
         q_gain[None, :],
         k_gain[None, :],
-        rotation_freqs(head_size),
         tokens,
         ffn_gain[None, :],
         route.T,
@@ -635,6 +710,13 @@
         down_weight,
         out_weight,
     )
+    return pl.pallas_call(
+        store_kernel,
+        out_shape=tuple(jax.ShapeDtypeStruct(part.shape, bf16) for part in held),
+        in_specs=[vmem] * len(held),
+        out_specs=(hbm,) * len(held),
+        scratch_shapes=[dma((len(held),))],
+    )(*[pltpu.with_memory_space_constraint(part, pltpu.VMEM) for part in held])
 
 
 GROUPS = 4
@@ -646,7 +728,8 @@
     cap = 2 * tokens.shape[0] * route.shape[1] // ep
     fits = (
         tp == 4
-        and ep % 2 == 0
+        and ep == 8
+        and queries.shape[1] % (2 * q_gain.shape[0]) == 0
         and ep % GROUPS == 0
         and cap % 16 == 0
         and keys.shape[1] == q_gain.shape[0]

time: 65.8 us -> 48.6 us (0.74)
  Pallas kernels: 60.9 us -> 47.1 us
  local copies, waits for them, and re-layouts: 3.93 us -> 0 us
    pallas_call x1, Pallas kernels: 60.9 us -> 46.3 us  [local_fused(): pl.pallas_call(functools.partial(fused_kernel, (ep, tp, cap, groups, tile...]
    unnamed x2 -> x0, local copies, waits for them, and re-layouts: 3.24 us -> none
    pallas_call x0 -> x1, Pallas kernels: none -> 0.76 us  [local_fused(): pl.pallas_call(store_kernel, out_shape=tuple((jax.ShapeDtypeStruct(part.s...]
where the time goes in v1:
time: 48.6 us; the launch traced here: 47.9 us
  Pallas kernels  47.1 us (97%)
  between operations  0.8 us (2%)
    pallas_call x1, Pallas kernels, local_fused(): pl.pallas_call(functools.partial(fused_kernel, (ep, tp, cap, groups, tile...  46.3 us

profile of v1, /device:TPU:0, one launch (start us, length us, event | category | flops | bytes accessed | tf_op | source)
XLA Modules:
  0.0 47.9 jit_solution(8318589577234822850)
XLA Ops:
  0.6 46.3 %shard_map.140 = (bf16[64,2048]{1,0:T(8,128)(2,1)S(1)}, bf16[32,2048]{1,0:T(8,128)(2,1)S(1)}) custom-call(bf16[256,256]{1,0:T(8,128)(2,1)} %q_ref.1, bf16[64,256]{1,0:T(8,128)(2,1)} %bitcast.7, bf16[64,256]{1,0:T(8,128)(2,1)} %bitcast.8, f32[1,64]{1,0:T(1,128)} %bitcast.12, f32[1,64]{1,0:T(1,128)} %bitcast.13, bf16[32,2048]{1,0:T(8,128)(2,1)} %tok_ref.1, ...), custom_call_target="tpu_custom_call" | custom-call | flops 6174015488 | bytes 11010048 | tf_op jit(solution)/shard_map/pallas_call | solution.py:655
  47.0 0.8 %shard_map.141 = (bf16[64,2048]{1,0:T(8,128)(2,1)}, bf16[32,2048]{1,0:T(8,128)(2,1)}) custom-call(bf16[64,2048]{1,0:T(8,128)(2,1)S(1)} %get-tuple-element.4.mix_ref, bf16[32,2048]{1,0:T(8,128)(2,1)S(1)} %get-tuple-element.5.rows_ref), custom_call_target="tpu_custom_call" | custom-call | tf_op jit(solution)/shard_map/pallas_call | solution.py:713

commit v2 on v1

--- a/solution.py
+++ b/solution.py
@@ -209,6 +209,7 @@
     mrs1,
     mhalf,
     mrs2,
+    passing,
     w_sem,
     a2a_s,
     a2a_r,
@@ -232,6 +233,8 @@
     m1_r,
     m2_s,
     m2_r,
+    y2_s,
+    y2_r,
 ):
     ep, tp, cap, groups, tile = dims
     f32, bf16 = jnp.float32, jnp.bfloat16
@@ -267,6 +270,9 @@
             device_id_type=pl.DeviceIdType.MESH,
         )
 
+    def landed(ref, sem):
+        pltpu.make_async_copy(ref, ref, sem).wait()
+
     barrier = pltpu.get_barrier_semaphore()
     peers = [(peer(mask), t) for mask in range(1, ep)] + [(e, t1), (e, t2)]
     for pe, pt in peers:
@@ -274,26 +280,15 @@
             barrier, inc=1, device_id={"ep": pe, "tp": pt}, device_id_type=pl.DeviceIdType.MESH
         )
 
-    weights = []
     for n in range(units // lane_tile):
         cols = pl.ds(n * lane_tile, lane_tile)
-        weights.append(
+        for side, source in ((0, gate_hbm), (lane_tile, up_hbm)):
             pltpu.make_async_copy(
-                gate_hbm.at[0, :, cols], wgu.at[n, :, pl.ds(0, lane_tile)], w_sem.at[2 * n]
-            )
-        )
-        weights.append(
-            pltpu.make_async_copy(
-                up_hbm.at[0, :, cols],
-                wgu.at[n, :, pl.ds(lane_tile, lane_tile)],
-                w_sem.at[2 * n + 1],
-            )
-        )
-    last = 2 * (units // lane_tile)
-    weights.append(pltpu.make_async_copy(down_hbm.at[0], wd, w_sem.at[last]))
-    load_out = pltpu.make_async_copy(ow_hbm, wo, w_sem.at[last + 1])
-    for copy in weights:
-        copy.start()
+                source.at[0, :, cols], wgu.at[n, :, pl.ds(side, lane_tile)], w_sem.at[0]
+            ).start()
+    load_down = pltpu.make_async_copy(down_hbm.at[0], wd, w_sem.at[1])
+    load_out = pltpu.make_async_copy(ow_hbm, wo, w_sem.at[2])
+    load_down.start()
     load_out.start()
 
     slot_rows = ep * cap
@@ -313,6 +308,7 @@
             spot += jnp.where(expert == peer(mask), place[mask], 0)
         return spot
 
+    mix_weights = [column(rw_ref[k : k + 1, :]) for k in range(topk)]
     columns = [column(route_t_ref[k : k + 1, :]) for k in range(topk)]
     for k in range(topk):
         col = columns[k]
@@ -345,26 +341,41 @@
     with jax.named_scope("barrier"):
         pl.semaphore_wait(barrier, len(peers))
 
-    a2a, f1, f2, f3 = {}, {}, {}, {}
+    a2a, f1, f2, f3, y2 = {}, {}, {}, {}, {}
     for i in range(ep):
         g, m = i // per, i % per
         if order[i]:
             a2a[i] = remote(
-                og.at[i], slots.at[g, 0, m], a2a_s.at[i], a2a_r.at[i], peer(order[i]), t
+                og.at[i], slots.at[g, 0, m], a2a_s, a2a_r.at[i], peer(order[i]), t
             )
-        f1[i] = remote(slots.at[g, 0, m], slots.at[g, 1, m], f1_s.at[i], f1_r.at[i], e, t1)
-        f2[i] = remote(slots.at[g, 0, m], slots.at[g, 2, m], f2_s.at[i], f2_r.at[i], e, t2)
-        f3[i] = remote(slots.at[g, 2, m], slots.at[g, 3, m], f3_s.at[i], f3_r.at[i], e, t1)
+        f1[i] = remote(slots.at[g, 0, m], slots.at[g, 1, m], f1_s, f1_r.at[g], e, t1)
+        mask = order[i]
+        if 0 < mask < half_ep:
+            f2[i] = remote(og.at[i], passing.at[mask], f2_s, f2_r.at[i], e, t2)
+            y2[i] = remote(
+                passing.at[mask], slots.at[g, 2, m], y2_s, y2_r.at[mask], peer(mask), t
+            )
+        else:
+            f2[i] = remote(slots.at[g, 0, m], slots.at[g, 2, m], f2_s, f2_r.at[i], e, t2)
+        f3[i] = remote(slots.at[g, 2, m], slots.at[g, 3, m], f3_s, f3_r.at[g], e, t1)
     kva, kvb = {}, {}
     for k in range(half_ep):
-        kvb[k] = remote(kvs.at[0, k], kvs.at[1, k], kvb_s.at[k], kvb_r.at[k], peer(1), t)
-        if k:
+        kvb[k] = remote(kvs.at[0, k], kvs.at[1, k], kvb_s, kvb_r, peer(1), t)
+        if k in (1, 2):
             kva[k] = remote(
-                kvs.at[0, 0], kvs.at[0, k], kva_s.at[k], kva_r.at[k], peer(2 * k), t
+                kvs.at[0, 0], kvs.at[0, k], kva_s, kva_r.at[k], peer(2 * k), t
+            )
+        if k == 3:
+            kva[k] = remote(
+                kvs.at[0, 2], kvs.at[0, 3], kva_s, kva_r.at[k], peer(2), t
             )
 
     near, far = issue_order(ep)
     for mask in near:
+        a2a[place[mask]].start()
+    for mask in range(1, half_ep):
+        f2[place[mask]].start()
+    for mask in far:
         a2a[place[mask]].start()
 
     def forward(mask):
@@ -372,13 +383,20 @@
         with jax.named_scope(f"fwd{mask}"):
             if mask:
                 a2a[i].wait_recv()
-            f2[i].start()
+            if not 0 < mask < half_ep:
+                f2[i].start()
             f1[i].start()
+
+    def pass_on(mask):
+        i = place[mask]
+        with jax.named_scope(f"pass{mask}"):
+            f2[i].wait_recv()
+            y2[i].start()
 
     def relay(mask):
         i = place[mask]
         with jax.named_scope(f"relay{mask}"):
-            f2[i].wait_recv()
+            (y2[i] if 0 < mask < half_ep else f2[i]).wait_recv()
             f3[i].start()
 
     forward(0)
@@ -398,10 +416,6 @@
     kvs[0, 0, :, pl.ds(0, head_size)] = rot_k.astype(bf16)
     kvs[0, 0, :, pl.ds(head_size, head_size)] = both[:, head_size:].astype(bf16)
 
-    for mask in far:
-        a2a[place[mask]].start()
-    for copy in kva.values():
-        copy.start()
     kvb[0].start()
 
     for h in range(heads):
@@ -413,6 +427,8 @@
     def share_keys(k):
         with jax.named_scope(f"share{k}"):
             kva[k].wait_recv()
+            if k == 2:
+                kva[3].start()
             kvb[k].start()
 
     scale = head_size ** (-0.5) * math.log2(math.e)
@@ -442,7 +458,7 @@
     mrows = rows // tp
     homes = [t, t1, t2, (t1 + 2) % tp]
     m1 = [
-        remote(mpart.at[2 * i + 1], mrs1.at[i], m1_s.at[i], m1_r.at[i], e, t1) for i in range(2)
+        remote(mpart.at[2 * i + 1], mrs1.at[i], m1_s, m1_r.at[i], e, t1) for i in range(2)
     ]
     m2 = remote(mhalf, mrs2, m2_s, m2_r, e, t2)
 
@@ -455,9 +471,8 @@
 
     def feed_wait(g):
         with jax.named_scope(f"feedwait{g}"):
-            for i in range(g * per, (g + 1) * per):
-                f1[i].wait_recv()
-                f3[i].wait_recv()
+            landed(slots.at[g, 1], f1_r.at[g])
+            landed(slots.at[g, 3], f3_r.at[g])
 
     rows_g = tp * per * cap
 
@@ -483,14 +498,14 @@
     for g in range(groups):
         for i in range(2):
             r1[g, i] = remote(
-                part.at[g, 2 * i + 1], rs1.at[g, i], r1_s.at[g, i], r1_r.at[g, i], e, t1
+                part.at[g, 2 * i + 1], rs1.at[g, i], r1_s, r1_r.at[g, i], e, t1
             )
-        r2[g] = remote(half.at[g], rs2.at[g], r2_s.at[g], r2_r.at[g], e, t2)
+        r2[g] = remote(half.at[g], rs2.at[g], r2_s, r2_r.at[g], e, t2)
     bk = {}
     for i in range(ep):
         if order[i]:
             bk[i] = remote(
-                home.at[i // per, i % per], back.at[i], bk_s.at[i], bk_r.at[i], peer(order[i]), t
+                home.at[i // per, i % per], back.at[i], bk_s, bk_r, peer(order[i]), t
             )
 
     def pair_sum(g):
@@ -519,93 +534,103 @@
             mhalf[...] = (mpart[2].astype(f32) + mrs1[1].astype(f32)).astype(bf16)
             m2.start()
 
+    kva[2].start()
+    pass_on(1)
     forward(1)
+    pass_on(2)
+    pass_on(3)
+    kva[1].start()
+    relay(1)
+    forward(4)
     forward(2)
+    forward(3)
     relay(0)
-    relay(1)
-    forward(3)
-    forward(4)
-    relay(2)
-    for copy in weights:
-        copy.wait()
+    pltpu.make_async_copy(wgu, wgu, w_sem.at[0]).wait()
+    load_down.wait()
+    relay(4)
+    forward(5)
     feed_wait(0)
     up(0)
+    relay(2)
+    forward(6)
     down(0)
-    relay(3)
-    forward(5)
-    relay(4)
-    forward(6)
     forward(7)
+    relay(5)
     feed_wait(1)
-    share_keys(1)
+    share_keys(2)
     up(1)
     pair_sum(0)
-    relay(5)
+    relay(3)
+    relay(6)
     down(1)
-    relay(6)
-    share_keys(2)
+    relay(7)
+    share_keys(1)
     feed_wait(2)
     up(2)
-    relay(7)
+    share_keys(3)
     pair_sum(1)
     down(2)
-    share_keys(3)
     feed_wait(3)
     up(3)
+    finish(0)
     pair_sum(2)
     down(3)
-    finish(0)
-    pair_sum(3)
     with jax.named_scope("kvwait"):
-        for k in range(half_ep):
-            kvb[k].wait_recv()
+        landed(kvs.at[1], kvb_r)
     with jax.named_scope("att0"):
         attend(1 - y, 0)
+    pair_sum(3)
     finish(1)
     with jax.named_scope("att1"):
         attend(1 - y, 2)
     load_out.wait()
     with jax.named_scope("project"):
         project((3, 2))
-    finish(2)
     with jax.named_scope("att2"):
         attend(y, 0)
     mixer_half()
+    finish(2)
     with jax.named_scope("att3"):
         attend(y, 2)
-    finish(3)
     with jax.named_scope("project"):
         project((1, 0))
+    finish(3)
+    others = pl.ds(0, ep - 1)
+    landed(og.at[others], a2a_s)
+    for sem in (f1_s, f2_s, f3_s):
+        landed(og, sem)
+    landed(og.at[pl.ds(0, half_ep - 1)], y2_s)
+    landed(kvs.at[0, pl.ds(0, half_ep - 1)], kva_s)
+    landed(kvs.at[0], kvb_s)
+    landed(rs1, r1_s)
+    landed(rs2, r2_s)
+    with jax.named_scope("bkwait"):
+        landed(back.at[pl.ds(0, ep - 1)], bk_r)
+    returned = back[...].reshape(slot_rows, width)
+    chosen = jnp.dot(jnp.concatenate(picks, axis=0), returned, preferred_element_type=f32)
+    mixed = jnp.zeros((own_rows, width), f32)
+    for k in range(topk):
+        mixed += mix_weights[k] * chosen[k * own_rows : (k + 1) * own_rows]
+    out_ref[...] = mixed.astype(bf16)
     with jax.named_scope("mwait"):
         m1[0].wait_recv()
         m2.wait_recv()
     mix_ref[...] = (
         mpart[0].astype(f32) + mrs1[0].astype(f32) + mrs2[...].astype(f32)
     ).astype(bf16)
-    with jax.named_scope("bkwait"):
-        for copy in bk.values():
-            copy.wait_recv()
-    returned = back[...].reshape(slot_rows, width)
-    mixed = jnp.zeros((own_rows, width), f32)
-    for k in range(topk):
-        mixed += column(rw_ref[k : k + 1, :]) * jnp.dot(
-            picks[k], returned, preferred_element_type=f32
-        )
-    out_ref[...] = mixed.astype(bf16)
-
-    for group in (kva, kvb, a2a, f1, f2, f3, r1, r2, bk):
-        for copy in group.values():
-            copy.wait_send()
-    for copy in m1 + [m2]:
-        copy.wait_send()
+    landed(og.at[others], bk_s)
+    landed(mrs1, m1_s)
+    m2.wait_send()
 
 
 def peer_order(ep):
-    return tuple(range(1, ep)) + (0,)
+    half = ep // 2
+    near = tuple(range(1, half)) + (0,)
+    return tuple(m for i, k in enumerate(near) for m in (k, half + i))
 
 
 def issue_order(ep):
-    return tuple(range(1, ep)), ()
+    return (1, 2, 3), tuple(range(4, ep))
 
 
 def store_kernel(mix_ref, rows_ref, mix_out, rows_out, sems):
@@ -680,15 +705,14 @@
             pltpu.VMEM((2, mrows, width), bf16),
             pltpu.VMEM((mrows, width), bf16),
             pltpu.VMEM((mrows, width), bf16),
-            dma((2 * (units // lane_tile) + 2,)),
+            pltpu.VMEM((ep // 2, cap, width), bf16),
+            dma((3,)),
         ]
-        + [dma((ep,))] * 8
-        + [dma((ep // 2,))] * 4
-        + [dma((groups, 2))] * 2
-        + [dma((groups,))] * 2
-        + [dma((ep,))] * 2
-        + [dma((2,))] * 2
-        + [dma, dma],
+        + [dma, dma((ep,)), dma, dma((groups,)), dma, dma((ep,)), dma, dma((groups,))]
+        + [dma, dma((ep // 2,)), dma, dma]
+        + [dma, dma((groups, 2)), dma, dma((groups,)), dma, dma]
+        + [dma, dma((2,)), dma, dma]
+        + [dma, dma((ep // 2,))],
         compiler_params=pltpu.CompilerParams(
             collective_id=0, has_side_effects=True, vmem_limit_bytes=60 * 1024 * 1024
         ),

time: 48.6 us -> 45.9 us (0.944); the launches traced: 47.9 us -> 45.7 us
  Pallas kernels: 47.1 us -> 44.9 us
    pallas_call x1, Pallas kernels: 46.3 us -> 44.1 us  [local_fused(): pl.pallas_call(functools.partial(fused_kernel, (ep, tp, cap, groups, tile...]
where the time goes in v2:
time: 45.9 us; the launch traced here: 45.7 us
  Pallas kernels  44.9 us (98%)
  between operations  0.8 us (2%)
    pallas_call x1, Pallas kernels, local_fused(): pl.pallas_call(functools.partial(fused_kernel, (ep, tp, cap, groups, tile...  44.1 us

profile of v2, /device:TPU:0, one launch (start us, length us, event | category | flops | bytes accessed | tf_op | source)
XLA Modules:
  0.0 45.7 jit_solution(11146525024196789071)
XLA Ops:
  0.6 44.1 %shard_map.140 = (bf16[64,2048]{1,0:T(8,128)(2,1)S(1)}, bf16[32,2048]{1,0:T(8,128)(2,1)S(1)}) custom-call(bf16[256,256]{1,0:T(8,128)(2,1)} %q_ref.1, bf16[64,256]{1,0:T(8,128)(2,1)} %bitcast.7, bf16[64,256]{1,0:T(8,128)(2,1)} %bitcast.8, f32[1,64]{1,0:T(1,128)} %bitcast.12, f32[1,64]{1,0:T(1,128)} %bitcast.13, bf16[32,2048]{1,0:T(8,128)(2,1)} %tok_ref.1, ...), custom_call_target="tpu_custom_call" | custom-call | flops 6174015488 | bytes 11010048 | tf_op jit(solution)/shard_map/pallas_call | solution.py:680
  44.8 0.8 %shard_map.141 = (bf16[64,2048]{1,0:T(8,128)(2,1)}, bf16[32,2048]{1,0:T(8,128)(2,1)}) custom-call(bf16[64,2048]{1,0:T(8,128)(2,1)S(1)} %get-tuple-element.4.mix_ref, bf16[32,2048]{1,0:T(8,128)(2,1)S(1)} %get-tuple-element.5.rows_ref), custom_call_target="tpu_custom_call" | custom-call | tf_op jit(solution)/shard_map/pallas_call | solution.py:737

commit v3 on v2

--- a/solution.py
+++ b/solution.py
@@ -175,6 +175,21 @@
 
 def fused_kernel(
     dims,
+    q_hbm,
+    k_hbm,
+    v_hbm,
+    qg_hbm,
+    kg_hbm,
+    tok_hbm,
+    fg_hbm,
+    route_hbm,
+    rw_hbm,
+    gate_hbm,
+    up_hbm,
+    down_hbm,
+    ow_hbm,
+    mix_ref,
+    out_ref,
     q_ref,
     k_ref,
     v_ref,
@@ -184,12 +199,6 @@
     fg_ref,
     route_t_ref,
     rw_ref,
-    gate_hbm,
-    up_hbm,
-    down_hbm,
-    ow_hbm,
-    mix_ref,
-    out_ref,
     wgu,
     wd,
     wo,
@@ -210,6 +219,7 @@
     mhalf,
     mrs2,
     passing,
+    in_sem,
     w_sem,
     a2a_s,
     a2a_r,
@@ -280,6 +290,33 @@
             barrier, inc=1, device_id={"ep": pe, "tp": pt}, device_id_type=pl.DeviceIdType.MESH
         )
 
+    routed = [
+        pltpu.make_async_copy(source, target, in_sem.at[n])
+        for n, (source, target) in enumerate(
+            (
+                (route_hbm, route_t_ref),
+                (tok_hbm, tok_ref),
+                (fg_hbm, fg_ref),
+                (rw_hbm, rw_ref),
+            )
+        )
+    ]
+    attended = [
+        pltpu.make_async_copy(source, target, in_sem.at[len(routed) + n])
+        for n, (source, target) in enumerate(
+            (
+                (k_hbm, k_ref),
+                (v_hbm, v_ref),
+                (kg_hbm, kg_ref),
+                (qg_hbm, qg_ref),
+                (q_hbm, q_ref),
+            )
+        )
+    ]
+    for copy in routed + attended:
+        copy.start()
+    for copy in routed + attended:
+        copy.wait()
     for n in range(units // lane_tile):
         cols = pl.ds(n * lane_tile, lane_tile)
         for side, source in ((0, gate_hbm), (lane_tile, up_hbm)):
@@ -677,15 +714,27 @@
     dma = pltpu.SemaphoreType.DMA
     mrows = rows // tp
     flops = 2 * tp * ep * cap * width * units * 3 + 4 * heads * rows * rows * ep * head_size
+    loaded = (
+        queries,
+        keys.T,
+        values.T,
+        q_gain[None, :],
+        k_gain[None, :],
+        tokens,
+        ffn_gain[None, :],
+        route.T,
+        route_weight.T,
+    )
     held = pl.pallas_call(
         functools.partial(fused_kernel, (ep, tp, cap, groups, tile)),
         out_shape=(
             pltpu.VMEM((mrows, width), bf16),
             pltpu.VMEM((own_rows, width), bf16),
         ),
-        in_specs=[vmem] * 9 + [hbm] * 4,
+        in_specs=[hbm] * 13,
         out_specs=(vmem, vmem),
-        scratch_shapes=[
+        scratch_shapes=[pltpu.VMEM(part.shape, part.dtype) for part in loaded]
+        + [
             pltpu.VMEM((units // lane_tile, width, 2 * lane_tile), bf16),
             pltpu.VMEM((units, width), bf16),
             pltpu.VMEM(out_weight.shape, bf16),
@@ -706,6 +755,7 @@
             pltpu.VMEM((mrows, width), bf16),
             pltpu.VMEM((mrows, width), bf16),
             pltpu.VMEM((ep // 2, cap, width), bf16),
+            dma((len(loaded),)),
             dma((3,)),
         ]
         + [dma, dma((ep,)), dma, dma((groups,)), dma, dma((ep,)), dma, dma((groups,))]
@@ -720,15 +770,7 @@
             flops=flops, bytes_accessed=3 * 2 * width * units, transcendentals=0
         ),
     )(
-        queries,
-        keys.T,
-        values.T,
-        q_gain[None, :],
-        k_gain[None, :],
-        tokens,
-        ffn_gain[None, :],
-        route.T,
-        route_weight.T,
+        *loaded,
         gate_weight,
         up_weight,
         down_weight,

time: 45.9 us -> 45 us (0.980)
  Pallas kernels: 44.9 us -> 44 us
    pallas_call x1, Pallas kernels: 44.1 us -> 43.2 us  [local_fused(): pl.pallas_call(functools.partial(fused_kernel, (ep, tp, cap, groups, tile...]
where the time goes in v3:
time: 45 us; the launch traced here: 44.8 us
  Pallas kernels  44 us (98%)
  between operations  0.8 us (2%)
    pallas_call x1, Pallas kernels, local_fused(): pl.pallas_call(functools.partial(fused_kernel, (ep, tp, cap, groups, tile...  43.2 us

profile of v3, /device:TPU:0, one launch (start us, length us, event | category | flops | bytes accessed | tf_op | source)
XLA Modules:
  0.0 44.8 jit_solution(12213025055688118310)
XLA Ops:
  0.6 43.2 %shard_map.140 = (bf16[64,2048]{1,0:T(8,128)(2,1)S(1)}, bf16[32,2048]{1,0:T(8,128)(2,1)S(1)}) custom-call(bf16[256,256]{1,0:T(8,128)(2,1)} %q_hbm.1, bf16[64,256]{1,0:T(8,128)(2,1)} %bitcast.7, bf16[64,256]{1,0:T(8,128)(2,1)} %bitcast.8, f32[1,64]{1,0:T(1,128)} %bitcast.12, f32[1,64]{1,0:T(1,128)} %bitcast.13, bf16[32,2048]{1,0:T(8,128)(2,1)} %tok_hbm.1, ...), custom_call_target="tpu_custom_call" | custom-call | flops 6174015488 | bytes 11010048 | tf_op jit(solution)/shard_map/pallas_call | solution.py:728
  43.9 0.8 %shard_map.141 = (bf16[64,2048]{1,0:T(8,128)(2,1)}, bf16[32,2048]{1,0:T(8,128)(2,1)}) custom-call(bf16[64,2048]{1,0:T(8,128)(2,1)S(1)} %get-tuple-element.4.mix_ref, bf16[32,2048]{1,0:T(8,128)(2,1)S(1)} %get-tuple-element.5.rows_ref), custom_call_target="tpu_custom_call" | custom-call | tf_op jit(solution)/shard_map/pallas_call | solution.py:779

commit v4 on v3

--- a/solution.py
+++ b/solution.py
@@ -594,9 +594,9 @@
     forward(7)
     relay(5)
     feed_wait(1)
+    pair_sum(0)
     share_keys(2)
     up(1)
-    pair_sum(0)
     relay(3)
     relay(6)
     down(1)

time: 45 us -> 44.7 us (level)
  no operation moved by 1% of the time
where the time goes in v4:
time: 44.7 us; the launch traced here: 44.5 us
  Pallas kernels  43.7 us (98%)
  between operations  0.8 us (2%)
    pallas_call x1, Pallas kernels, local_fused(): pl.pallas_call(functools.partial(fused_kernel, (ep, tp, cap, groups, tile...  42.9 us

profile of v4, /device:TPU:0, one launch (start us, length us, event | category | flops | bytes accessed | tf_op | source)
XLA Modules:
  0.0 44.5 jit_solution(12734116577082297370)
XLA Ops:
  0.6 42.9 %shard_map.140 = (bf16[64,2048]{1,0:T(8,128)(2,1)S(1)}, bf16[32,2048]{1,0:T(8,128)(2,1)S(1)}) custom-call(bf16[256,256]{1,0:T(8,128)(2,1)} %q_hbm.1, bf16[64,256]{1,0:T(8,128)(2,1)} %bitcast.7, bf16[64,256]{1,0:T(8,128)(2,1)} %bitcast.8, f32[1,64]{1,0:T(1,128)} %bitcast.12, f32[1,64]{1,0:T(1,128)} %bitcast.13, bf16[32,2048]{1,0:T(8,128)(2,1)} %tok_hbm.1, ...), custom_call_target="tpu_custom_call" | custom-call | flops 6174015488 | bytes 11010048 | tf_op jit(solution)/shard_map/pallas_call | solution.py:728
  43.6 0.8 %shard_map.141 = (bf16[64,2048]{1,0:T(8,128)(2,1)}, bf16[32,2048]{1,0:T(8,128)(2,1)}) custom-call(bf16[64,2048]{1,0:T(8,128)(2,1)S(1)} %get-tuple-element.4.mix_ref, bf16[32,2048]{1,0:T(8,128)(2,1)S(1)} %get-tuple-element.5.rows_ref), custom_call_target="tpu_custom_call" | custom-call | tf_op jit(solution)/shard_map/pallas_call | solution.py:779

commit v5 on v4

--- a/solution.py
+++ b/solution.py
@@ -705,7 +705,7 @@
     cap = 2 * own_rows * route.shape[1] // ep
     units = gate_weight.shape[2]
     lane_tile = 128
-    tile = math.gcd(width, 512)
+    tile = math.gcd(width, 1024)
     groups = GROUPS
     per = ep // groups
     bf16 = jnp.bfloat16

time: 44.7 us -> 44.7 us (level)
  no operation moved by 1% of the time
where the time goes in v5:
time: 44.7 us; the launch traced here: 44.5 us
  Pallas kernels  43.7 us (98%)
  between operations  0.8 us (2%)
    pallas_call x1, Pallas kernels, local_fused(): pl.pallas_call(functools.partial(fused_kernel, (ep, tp, cap, groups, tile...  42.9 us

profile of v5, /device:TPU:0, one launch (start us, length us, event | category | flops | bytes accessed | tf_op | source)
XLA Modules:
  0.0 44.5 jit_solution(1074894505649613778)
XLA Ops:
  0.6 42.9 %shard_map.140 = (bf16[64,2048]{1,0:T(8,128)(2,1)S(1)}, bf16[32,2048]{1,0:T(8,128)(2,1)S(1)}) custom-call(bf16[256,256]{1,0:T(8,128)(2,1)} %q_hbm.1, bf16[64,256]{1,0:T(8,128)(2,1)} %bitcast.7, bf16[64,256]{1,0:T(8,128)(2,1)} %bitcast.8, f32[1,64]{1,0:T(1,128)} %bitcast.12, f32[1,64]{1,0:T(1,128)} %bitcast.13, bf16[32,2048]{1,0:T(8,128)(2,1)} %tok_hbm.1, ...), custom_call_target="tpu_custom_call" | custom-call | flops 6174015488 | bytes 11010048 | tf_op jit(solution)/shard_map/pallas_call | solution.py:728
  43.6 0.8 %shard_map.141 = (bf16[64,2048]{1,0:T(8,128)(2,1)}, bf16[32,2048]{1,0:T(8,128)(2,1)}) custom-call(bf16[64,2048]{1,0:T(8,128)(2,1)S(1)} %get-tuple-element.4.mix_ref, bf16[32,2048]{1,0:T(8,128)(2,1)S(1)} %get-tuple-element.5.rows_ref), custom_call_target="tpu_custom_call" | custom-call | tf_op jit(solution)/shard_map/pallas_call | solution.py:779
